TPU v7x, 32 devices: a whole 2x2x4 slice. The times are simulated.
32 devices in a mesh: ep: 4 (over z), tp: 8 (over y, x, core).
Axes of the slice: x: 2, y: 2, z: 4, core: 2. Of those that a mesh axis runs over, the one named last changes fastest.
Arguments:
- tokens: bfloat16 [32, 4096], P('ep'), may hold values from -6 to 6
- norm_gains: float32 [4, 4096], replicated, may hold values from 0.1 to 1.9
- w_query: bfloat16 [4096, 4096], P(None, 'tp'), may hold values from -0.09375 to 0.09375
- w_query_rope: bfloat16 [4096, 2048], P(None, 'tp'), may hold values from -0.09375 to 0.09375
- w_key_up: bfloat16 [32, 128, 1024], P('tp'), may hold values from -0.5 to 0.5
- w_value_up: bfloat16 [32, 1024, 128], P('tp'), may hold values from -0.1875 to 0.1875
- w_output: bfloat16 [4096, 4096], P('tp'), may hold values from -0.09375 to 0.09375
- w_latent_down: bfloat16 [4096, 1024], P(None, 'tp'), may hold values from -0.09375 to 0.09375
- latent_gain: float32 [1024], replicated, may hold values from 0.1 to 1.9
- w_rope_down: bfloat16 [4096, 64], replicated, may hold values from -0.09375 to 0.09375
- cache_latent: bfloat16 [32, 1024, 1024], P(('ep', 'tp')), may hold values from -300 to 300
- cache_rope: bfloat16 [32, 1024, 64], P(('ep', 'tp')), may hold values from -6 to 6
- lengths: int32 [32], P(('ep', 'tp')), may hold values from 1 to 1024, as said below
- routes: int32 [32, 2], P('ep'), may hold values from 0 to 3, all different within a row; in each aligned block of 8 rows (0 to 7, 8 to 15, ...) at most 7 rows name the same one
- route_weights: float32 [32, 2], P('ep'), may hold values from 0.2 to 1
- w_gate: bfloat16 [4, 4096, 2048], P('ep', None, 'tp'), may hold values from -0.09375 to 0.09375
- w_up: bfloat16 [4, 4096, 2048], P('ep', None, 'tp'), may hold values from -0.09375 to 0.09375
- w_down: bfloat16 [4, 2048, 4096], P('ep', 'tp'), may hold values from -0.125 to 0.125
Outputs:
- hidden_out: bfloat16 [32, 4096], P(('ep', 'tp'))
- new_latent: bfloat16 [32, 1024], P(('ep', 'tp'))
- new_rope: bfloat16 [32, 64], P(('ep', 'tp'))
Inputs may be any that keep to these rules, and one draw needn't show every extreme that they name: `routes`: within each aligned block of 8 rows no expert is named by more than 7 rows, a bound that some block reaches; the 2 experts of a row differ. The new token stands at position lengths; some sequence has exactly 1024.
All inputs are finite; a program needn't handle non-finite values.
Results may differ from a plain program's by a relative error of at most 0.02.
Values may be sent and summed in bfloat16 or wider, within the bound.
A program may use at most 64 MiB of HBM per device.

v0:
```python
import jax
import jax.numpy as jnp
from jax import lax
from jax.sharding import PartitionSpec as P

EXP_LOCAL = 1


EPSILON = 1e-06
ROTARY_BASE = 500000.0


def rms_scale(source, gain_row):
    values_f = source.astype(jnp.float32)
    return (
        values_f
        * lax.rsqrt(jnp.mean(values_f * values_f, axis=-1, keepdims=True) + EPSILON)
        * gain_row
    )


def rotate(source, position):
    half_width = source.shape[-1] // 2
    frequency = ROTARY_BASE ** (-jnp.arange(half_width, dtype=jnp.float32) / half_width)
    angles = position[..., None] * frequency
    first_half = source[..., :half_width]
    second_half = source[..., half_width:]
    return jnp.concatenate(
        [
            first_half * jnp.cos(angles) - second_half * jnp.sin(angles),
            second_half * jnp.cos(angles) + first_half * jnp.sin(angles),
        ],
        axis=-1,
    )


def attend(q_latent, q_pe, cache_lat, cache_rp, lat_new, rope_new, lengths, score_scale):
    scores = (
        jnp.einsum("shc,spc->shp", q_latent, cache_lat, preferred_element_type=jnp.float32)
        + jnp.einsum("shr,spr->shp", q_pe, cache_rp, preferred_element_type=jnp.float32)
    ) * score_scale
    own_score = (
        jnp.einsum("shc,sc->sh", q_latent, lat_new, preferred_element_type=jnp.float32)
        + jnp.einsum("shr,sr->sh", q_pe, rope_new, preferred_element_type=jnp.float32)
    ) * score_scale
    visible = (
        jnp.arange(cache_lat.shape[1], dtype=jnp.int32)[None, None, :] < lengths[:, None, None]
    )
    row_max = jnp.maximum(jnp.max(jnp.where(visible, scores, -jnp.inf), axis=-1), own_score)
    weights = jnp.where(visible, jnp.exp(scores - row_max[..., None]), 0.0)
    own_weight = jnp.exp(own_score - row_max)
    denominator = jnp.sum(weights, axis=-1) + own_weight
    probabilities = (weights / denominator[..., None]).astype(jnp.bfloat16)
    own_prob = (own_weight / denominator).astype(jnp.bfloat16)
    attended = jnp.einsum(
        "shp,spc->shc", probabilities, cache_lat, preferred_element_type=jnp.float32
    )
    attended = (
        attended + own_prob.astype(jnp.float32)[..., None] * lat_new.astype(jnp.float32)[:, None, :]
    )
    return attended.astype(jnp.bfloat16)


def on_device(
    tokens,
    norm_gains,
    w_query,
    w_query_rope,
    w_key_up,
    w_value_up,
    w_output,
    w_latent_down,
    latent_gain,
    w_rope_down,
    cache_latent,
    cache_rope,
    lengths,
    routes,
    route_weights,
    w_gate,
    w_up,
    w_down,
):
    group_rows = tokens.shape[0]
    seq_count = cache_latent.shape[0]
    heads_here = w_key_up.shape[0]
    nope_width = w_key_up.shape[1]
    rope_width = w_rope_down.shape[1]
    tp_size = lax.axis_size("tp")
    tp_rank = lax.axis_index("tp")
    normed = rms_scale(tokens, norm_gains[0]).astype(jnp.bfloat16)
    q_nope = jnp.dot(normed, w_query, preferred_element_type=jnp.float32).astype(jnp.bfloat16)
    q_nope = q_nope.reshape(group_rows, heads_here, nope_width)
    q_latent = jnp.einsum("thn,hnc->thc", q_nope, w_key_up, preferred_element_type=jnp.float32)
    q_latent = q_latent.astype(jnp.bfloat16).reshape(group_rows, -1)
    q_rot = jnp.dot(normed, w_query_rope, preferred_element_type=jnp.float32).astype(jnp.bfloat16)
    latent_cols = jnp.dot(normed, w_latent_down, preferred_element_type=jnp.float32).astype(
        jnp.bfloat16
    )
    q_mine, rot_mine, latent_raw = (
        lax.all_to_all(q_latent, "tp", split_axis=0, concat_axis=1, tiled=True),
        lax.all_to_all(q_rot, "tp", split_axis=0, concat_axis=1, tiled=True),
        lax.all_to_all(latent_cols, "tp", split_axis=0, concat_axis=1, tiled=True),
    )
    heads_all = rot_mine.shape[1] // rope_width
    own_normed = lax.dynamic_slice_in_dim(normed, tp_rank * seq_count, seq_count, 0)
    rope_raw = jnp.dot(own_normed, w_rope_down, preferred_element_type=jnp.float32).astype(
        jnp.bfloat16
    )
    new_latent = rms_scale(latent_raw, latent_gain).astype(jnp.bfloat16)
    position = lengths.astype(jnp.float32)
    new_rope = rotate(rope_raw.astype(jnp.float32), position).astype(jnp.bfloat16)
    q_pe = rotate(
        rot_mine.reshape(seq_count, heads_all, rope_width).astype(jnp.float32), position[:, None]
    )
    q_pe = q_pe.astype(jnp.bfloat16)
    score_scale = (nope_width + rope_width) ** (-0.5)
    attended = attend(
        q_mine.reshape(seq_count, heads_all, -1),
        q_pe,
        cache_latent,
        cache_rope,
        new_latent,
        new_rope,
        lengths,
        score_scale,
    )
    head_latent = lax.all_to_all(
        attended.reshape(seq_count, -1), "tp", split_axis=1, concat_axis=0, tiled=True
    )
    values = (
        jnp.einsum(
            "thc,hcv->thv",
            head_latent.reshape(group_rows, heads_here, -1),
            w_value_up,
            preferred_element_type=jnp.float32,
        )
        .astype(jnp.bfloat16)
        .reshape(group_rows, -1)
    )
    head_term = jnp.dot(values, w_output, preferred_element_type=jnp.float32)
    mixed = lax.psum(head_term.astype(jnp.bfloat16), "tp").astype(jnp.float32)
    resid = (tokens.astype(jnp.float32) + rms_scale(mixed, norm_gains[1])).astype(jnp.bfloat16)
    expert_in = rms_scale(resid, norm_gains[2]).astype(jnp.bfloat16)
    own_resid = lax.dynamic_slice_in_dim(resid, tp_rank * seq_count, seq_count, 0)
    ep_size = lax.axis_size("ep")
    experts = ep_size * EXP_LOCAL
    local_expert = tp_rank // (tp_size // EXP_LOCAL)
    route_count = routes.shape[1]
    capacity = (
        (group_rows * route_count + experts - 1) // experts
        + 2
        + group_rows * route_count // (4 * experts)
    )
    slot_count = ep_size * capacity
    flat_routes = routes.reshape(-1)
    expert_hits = (flat_routes[:, None] == jnp.arange(experts, dtype=jnp.int32)[None, :]).astype(
        jnp.int32
    )
    slot_rank = jnp.sum((jnp.cumsum(expert_hits, axis=0) - 1) * expert_hits, axis=1)
    served_here = flat_routes % EXP_LOCAL == local_expert
    slot_index = jnp.where(served_here, flat_routes // EXP_LOCAL * capacity + slot_rank, -1)
    slot_picks = (slot_index[:, None] == jnp.arange(slot_count, dtype=jnp.int32)[None, :]).astype(
        jnp.bfloat16
    )
    slot_picks = slot_picks.reshape(group_rows, route_count, slot_count)
    slot_rows = jnp.sum(slot_picks, axis=1)
    outgoing = jnp.dot(slot_rows.T, expert_in, preferred_element_type=jnp.float32).astype(
        jnp.bfloat16
    )
    arrived = lax.all_to_all(outgoing, "ep", split_axis=0, concat_axis=0, tiled=True)
    gate_sum = jnp.dot(arrived, w_gate[0], preferred_element_type=jnp.float32)
    up_sum = jnp.dot(arrived, w_up[0], preferred_element_type=jnp.float32)
    hidden_units = (jax.nn.silu(gate_sum) * up_sum).astype(jnp.bfloat16)
    expert_out = jnp.dot(hidden_units, w_down[0], preferred_element_type=jnp.float32).astype(
        jnp.bfloat16
    )
    returned = lax.all_to_all(expert_out, "ep", split_axis=0, concat_axis=0, tiled=True)
    routed_part = jnp.zeros((group_rows, returned.shape[1]), jnp.float32)
    for route_slot in range(route_count):
        chosen = jnp.dot(slot_picks[:, route_slot, :], returned, preferred_element_type=jnp.float32)
        routed_part = routed_part + route_weights[:, route_slot : route_slot + 1] * chosen
    routed = lax.psum_scatter(
        routed_part.astype(jnp.bfloat16), "tp", scatter_dimension=0, tiled=True
    ).astype(jnp.float32)
    hidden_out = (own_resid.astype(jnp.float32) + rms_scale(routed, norm_gains[3])).astype(
        jnp.bfloat16
    )
    return (hidden_out, new_latent, new_rope)


def solution(mesh):
    in_specs = (
        P("ep", None),
        P(),
        P(None, "tp"),
        P(None, "tp"),
        P("tp", None, None),
        P("tp", None, None),
        P("tp", None),
        P(None, "tp"),
        P(),
        P(),
        P(("ep", "tp"), None, None),
        P(("ep", "tp"), None, None),
        P(("ep", "tp")),
        P("ep", None),
        P("ep", None),
        P("ep", None, "tp"),
        P("ep", None, "tp"),
        P("ep", "tp", None),
    )
    out_specs = (P(("ep", "tp"), None), P(("ep", "tp"), None), P(("ep", "tp"), None))
    return jax.shard_map(
        on_device, mesh=mesh, in_specs=in_specs, out_specs=out_specs, check_vma=False
    )
```

profile of v0, /device:TPU:0, one launch (start us, length us, event | category | flops | bytes accessed | tf_op | source)
XLA Modules:
  0.0 212.2 jit_solution(539098069489857588)
XLA Ops:
  7.2 1.1 fusion.78
  8.3 1.0 fusion.40
  9.3 0.9 fusion.42
  10.2 1.5 fusion.29
  11.7 0.6 copy.35
  12.3 5.2 %all-to-all-start.2 = ((bf16[8,1,128]{2,1,0:T(2,128)(2,1)}), bf16[8,1,128]{2,1,0:T(2,128)(2,1)S(1)}, u32[]{:S(2)}, u32[]{:S(2)}) async-start(bf16[8,1,128]{2,1,0:T(2,128)(2,1)} %copy.35), calls=%async_computation.2 | async-start | bytes 8192 | tf_op jit(solution)/shard_map/all_to_all | solution.py:103
  17.5 2.0 fusion.28
  20.2 1.3 fusion.34
  21.5 0.1 subtract_convert_fusion.1
  21.6 0.1 copy.38
  21.7 0.1 eq.42
  21.7 0.1 fusion.63
  21.8 0.2 select_reduce_fusion.1
  22.1 3.1 %convolution_convert_fusion.3 = bf16[4,8,1024]{2,1,0:T(8,128)(2,1)S(1)} fusion(bf16[4,128,1024]{2,1,0:T(8,128)(2,1)S(1)} %copy-done.2, bf16[8,4096]{1,0:T(8,128)(2,1)S(1)} %fusion.42, bf16[4096,512]{1,0:T(8,128)(2,1)} %param.20), kind=kOutput, calls=%fused_computation.20 | convolution fusion | flops 41979904 | bytes 5373952 | tf_op jit(solution)/shard_map/thn,hnc->thc/dot_general | solution.py:94
  25.1 0.5 broadcast.263
  25.7 0.6 reduce.13
  26.3 0.6 reshape.355
  26.9 0.7 reduce.12
  27.6 0.7 reshape.353
  28.2 0.1 reduce_sum.82
  28.3 4.2 %all-to-all-start.1 = ((bf16[8,2,128]{2,1,0:T(2,128)(2,1)}), bf16[8,2,128]{2,1,0:T(2,128)(2,1)S(1)}, u32[]{:S(2)}, u32[]{:S(2)}) async-start(bf16[8,2,128]{2,1,0:T(2,128)(2,1)} %reshape.355), calls=%async_computation.1 | async-start | bytes 8192 | tf_op jit(solution)/shard_map/all_to_all | solution.py:102
  32.5 0.6 multiply_reduce_fusion.1
  33.9 3.3 %all-to-all-done.1 = bf16[8,2,128]{2,1,0:T(2,128)(2,1)S(1)} async-done(((bf16[8,2,128]{2,1,0:T(2,128)(2,1)}), bf16[8,2,128]{2,1,0:T(2,128)(2,1)S(1)}, u32[]{:S(2)}, u32[]{:S(2)}) %all-to-all-start.1) | async-done | bytes 4128 | tf_op jit(solution)/shard_map/all_to_all | solution.py:102
  37.1 3.3 %all-to-all-start = ((bf16[8,2,2048]{2,1,0:T(2,128)(2,1)}), bf16[8,2,2048]{2,1,0:T(2,128)(2,1)S(1)}, u32[]{:S(2)}, u32[]{:S(2)}) async-start(bf16[8,2,2048]{2,1,0:T(2,128)(2,1)} %reshape.353), calls=%async_computation | async-start | bytes 131072 | tf_op jit(solution)/shard_map/all_to_all | solution.py:101
  40.5 0.1 reshape.340
  40.6 0.1 fusion.61
  40.7 4.8 %all-to-all-done = bf16[8,2,2048]{2,1,0:T(2,128)(2,1)S(1)} async-done(((bf16[8,2,2048]{2,1,0:T(2,128)(2,1)}), bf16[8,2,2048]{2,1,0:T(2,128)(2,1)S(1)}, u32[]{:S(2)}, u32[]{:S(2)}) %all-to-all-start) | async-done | bytes 65568 | tf_op jit(solution)/shard_map/all_to_all | solution.py:101
  45.5 0.4 reduce.7
  46.0 2.5 %fusion.9 = f32[32,1024]{1,0:T(8,128)S(1)} fusion(bf16[32,1024]{1,0:T(8,128)(2,1)S(1)} %reshape.334, bf16[1,1024,1024]{2,1,0:T(8,128)(2,1)} %param.28), kind=kOutput, calls=%fused_computation.14 | convolution fusion | flops 67108864 | bytes 2293760 | tf_op jit(solution)/shard_map/shc,spc->shp/dot_general | solution.py:39
  48.4 0.1 convolution_bitcast_fusion.2
  48.6 0.3 select_reduce_fusion
  48.9 0.2 fusion.79
  49.1 0.2 fusion.45
  49.3 0.5 fusion.15
  49.9 1.0 reduce.14
  50.9 0.7 reshape.357
  51.6 3.3 %all-to-all-start.3 = ((bf16[8,2,2048]{2,1,0:T(2,128)(2,1)}), bf16[8,2,2048]{2,1,0:T(2,128)(2,1)S(1)}, u32[]{:S(2)}, u32[]{:S(2)}) async-start(bf16[8,2,2048]{2,1,0:T(2,128)(2,1)} %reshape.357), calls=%async_computation.3 | async-start | bytes 131072 | tf_op jit(solution)/shard_map/all_to_all | solution.py:128
  55.0 0.1 copy.40
  55.1 4.8 %all-to-all-done.3 = bf16[8,2,2048]{2,1,0:T(2,128)(2,1)S(1)} async-done(((bf16[8,2,2048]{2,1,0:T(2,128)(2,1)}), bf16[8,2,2048]{2,1,0:T(2,128)(2,1)S(1)}, u32[]{:S(2)}, u32[]{:S(2)}) %all-to-all-start.3) | async-done | bytes 65568 | tf_op jit(solution)/shard_map/all_to_all | solution.py:128
  59.9 0.4 bitcast_reduce_fusion
  60.3 3.7 %convolution_convert_fusion.2 = bf16[8,4096]{1,0:T(8,128)(2,1)} fusion(bf16[512,4096]{1,0:T(8,128)(2,1)} %param.24, bf16[8,4,1024]{2,0,1:T(8,128)(2,1)S(1)} %bitcast.123, bf16[4,1024,128]{2,1,0:T(8,128)(2,1)S(1)} %copy-done.3), kind=kOutput, calls=%fused_computation.6 | convolution fusion | flops 41979904 | bytes 5373952 | tf_op jit(solution)/shard_map/dot_general | solution.py:141
  64.0 0.1 convert_reduce_fusion.1
  64.1 52.6 %all-reduce.4.cloned.1.call-done = bf16[8,4096]{1,0:T(8,128)(2,1)} async-done(((bf16[8,4096]{1,0:T(8,128)(2,1)}), bf16[8,4096]{1,0:T(8,128)(2,1)}) %all-reduce.4.cloned.1.call-update) | async-done | bytes 65552 | tf_op jit(solution)/shard_map/psum | solution.py:142
  116.7 1.0 fusion.35
  117.7 1.1 fusion.37
  118.8 0.3 convolution_convert_fusion.1
  119.1 0.1 all_to_all.64
  119.2 12.5 %all_to_all.77 = bf16[4,7,4096]{2,1,0:T(8,128)(2,1)S(1)} all-to-all(bf16[4,7,4096]{2,1,0:T(8,128)(2,1)S(1)} %all_to_all.64), channel_id=1, replica_groups=mesh['ep'=4,'tp'=8] {'ep'}, dimensions={0} | all-to-all | bytes 458752 | tf_op jit(solution)/shard_map/all_to_all | solution.py:171
  131.7 0.1 all_to_all.66
  131.8 2.1 fusion.5
  133.9 2.9 %convolution_convert_fusion = bf16[28,4096]{1,0:T(8,128)(2,1)S(1)} fusion(bf16[1,256,4096]{2,1,0:T(8,128)(2,1)S(1)} %copy-done, bf16[28,4096]{1,0:T(8,128)(2,1)S(1)} %all_to_all.66, bf16[1,4096,256]{2,1,0:T(8,128)(2,1)} %param.34, f32[28,256]{1,0:T(8,128)S(1)} %fusion.5), kind=kOutput, calls=%fused_computation | convolution fusion | flops 117598208 | bytes 4681728 | tf_op jit(solution)/shard_map/dot_general | solution.py:175
  136.7 0.8 all_to_all.67
  137.5 3.4 %all-to-all-start.5 = ((bf16[4,7,4096]{2,1,0:T(8,128)(2,1)}), bf16[4,7,4096]{2,1,0:T(8,128)(2,1)S(1)}, u32[]{:S(2)}, u32[]{:S(2)}) async-start(bf16[4,7,4096]{2,1,0:T(8,128)(2,1)} %all_to_all.67), calls=%async_computation.5 | async-start | bytes 524288 | tf_op jit(solution)/shard_map/all_to_all | solution.py:178
  141.0 0.1 iota_compare_fusion
  141.1 7.7 %all-to-all-done.5 = bf16[4,7,4096]{2,1,0:T(8,128)(2,1)S(1)} async-done(((bf16[4,7,4096]{2,1,0:T(8,128)(2,1)}), bf16[4,7,4096]{2,1,0:T(8,128)(2,1)S(1)}, u32[]{:S(2)}, u32[]{:S(2)}) %all-to-all-start.5) | async-done | bytes 229408 | tf_op jit(solution)/shard_map/all_to_all | solution.py:178
  148.8 0.1 all_to_all.69
  148.9 0.1 convolution_multiply_fusion.1
  149.1 0.8 fusion.1
  149.9 0.6 pad_maximum_fusion.3
  150.4 0.6 dynamic-slice
  151.0 0.6 convert_element_type.184
  151.6 48.9 %all-reduce.6.cloned.1.call-done = bf16[8,4096]{1,0:T(8,128)(2,1)} async-done(((bf16[8,4096]{1,0:T(8,128)(2,1)}), bf16[8,4096]{1,0:T(8,128)(2,1)}) %all-reduce.6.cloned.1.call-update) | async-done | bytes 65552
  200.5 2.0 multiply_reduce_fusion
  203.2 2.1 add_convert_fusion
  (43 shorter events, 0.6 us)
Async XLA Ops:
  7.2 126.7 %copy-start = (bf16[1,256,4096]{2,1,0:T(8,128)(2,1)S(1)}, bf16[1,256,4096]{2,1,0:T(8,128)(2,1)}, u32[]{:S(2)}) copy-start(bf16[1,256,4096]{2,1,0:T(8,128)(2,1)} %param.35) | copy-start | bytes 6291460
  7.2 14.4 %copy-start.7 = (s32[8,2]{0,1:T(2,128)S(1)}, s32[8,2]{0,1:T(2,128)}, u32[]{:S(2)}) copy-start(s32[8,2]{0,1:T(2,128)} %param.31) | copy-start | bytes 196
  7.2 14.8 %copy-start.2 = (bf16[4,128,1024]{2,1,0:T(8,128)(2,1)S(1)}, bf16[4,128,1024]{2,1,0:T(8,128)(2,1)}, u32[]{:S(2)}) copy-start(bf16[4,128,1024]{2,1,0:T(8,128)(2,1)} %param.22) | copy-start | bytes 3145732
  12.3 16.0 %all-to-all-start.2 = ((bf16[8,1,128]{2,1,0:T(2,128)(2,1)}), bf16[8,1,128]{2,1,0:T(2,128)(2,1)S(1)}, u32[]{:S(2)}, u32[]{:S(2)}) async-start(bf16[8,1,128]{2,1,0:T(2,128)(2,1)} %copy.35), calls=%async_computation.2 | async-start | bytes 8192 | tf_op jit(solution)/shard_map/all_to_all | solution.py:103
  22.0 11.8 %copy-start.6 = (f32[1024]{0:T(1024)S(1)}, f32[1024]{0:T(1024)}, u32[]{:S(2)}) copy-start(f32[1024]{0:T(1024)} %param.26) | copy-start | bytes 12292
  25.1 23.4 %copy-start.5 = (bf16[1,1024,64]{1,2,0:T(8,128)(2,1)S(1)}, bf16[1,1024,64]{1,2,0:T(8,128)(2,1)}, u32[]{:S(2)}) copy-start(bf16[1,1024,64]{1,2,0:T(8,128)(2,1)} %param.29) | copy-start | bytes 393220
  28.3 8.8 %all-to-all-start.1 = ((bf16[8,2,128]{2,1,0:T(2,128)(2,1)}), bf16[8,2,128]{2,1,0:T(2,128)(2,1)S(1)}, u32[]{:S(2)}, u32[]{:S(2)}) async-start(bf16[8,2,128]{2,1,0:T(2,128)(2,1)} %reshape.355), calls=%async_computation.1 | async-start | bytes 8192 | tf_op jit(solution)/shard_map/all_to_all | solution.py:102
  37.1 8.3 %all-to-all-start = ((bf16[8,2,2048]{2,1,0:T(2,128)(2,1)}), bf16[8,2,2048]{2,1,0:T(2,128)(2,1)S(1)}, u32[]{:S(2)}, u32[]{:S(2)}) async-start(bf16[8,2,2048]{2,1,0:T(2,128)(2,1)} %reshape.353), calls=%async_computation | async-start | bytes 131072 | tf_op jit(solution)/shard_map/all_to_all | solution.py:101
  45.9 3.4 %copy-start.1 = (bf16[1,1024,1024]{2,1,0:T(8,128)(2,1)S(1)}, bf16[1,1024,1024]{2,1,0:T(8,128)(2,1)}, u32[]{:S(2)}) copy-start(bf16[1,1024,1024]{2,1,0:T(8,128)(2,1)} %param.28) | copy-start | bytes 6291460
  48.4 11.9 %copy-start.3 = (bf16[4,1024,128]{2,1,0:T(8,128)(2,1)S(1)}, bf16[4,1024,128]{2,1,0:T(8,128)(2,1)}, u32[]{:S(2)}) copy-start(bf16[4,1024,128]{2,1,0:T(8,128)(2,1)} %param.23) | copy-start | bytes 3145732
  51.6 8.3 %all-to-all-start.3 = ((bf16[8,2,2048]{2,1,0:T(2,128)(2,1)}), bf16[8,2,2048]{2,1,0:T(2,128)(2,1)S(1)}, u32[]{:S(2)}, u32[]{:S(2)}) async-start(bf16[8,2,2048]{2,1,0:T(2,128)(2,1)} %reshape.357), calls=%async_computation.3 | async-start | bytes 131072 | tf_op jit(solution)/shard_map/all_to_all | solution.py:128
  54.9 61.8 %all-reduce.4.cloned.1.call-start = ((), (), s32[]{:S(2)}) async-start(), calls=%async_computation.6 | async-start | bytes 131072 | tf_op jit(solution)/shard_map/psum | solution.py:142
  60.3 57.4 %copy-start.4 = (bf16[8,4096]{1,0:T(8,128)(2,1)S(1)}, bf16[8,4096]{1,0:T(8,128)(2,1)}, u32[]{:S(2)}) copy-start(bf16[8,4096]{1,0:T(8,128)(2,1)} %param.18) | copy-start | bytes 196612
  133.8 7.1 %copy-start.8 = (f32[8,2]{0,1:T(2,128)S(1)}, f32[8,2]{0,1:T(2,128)}, u32[]{:S(2)}) copy-start(f32[8,2]{0,1:T(2,128)} %param.32) | copy-start | bytes 196
  136.7 13.7 %copy-start.9 = (u32[32]{0:T(128)S(1)}, u32[32]{0:T(128)}, u32[]{:S(2)}) copy-start(u32[32]{0:T(128)} %constant.96) | copy-start | bytes 388
  137.5 11.3 %all-to-all-start.5 = ((bf16[4,7,4096]{2,1,0:T(8,128)(2,1)}), bf16[4,7,4096]{2,1,0:T(8,128)(2,1)S(1)}, u32[]{:S(2)}, u32[]{:S(2)}) async-start(bf16[4,7,4096]{2,1,0:T(8,128)(2,1)} %all_to_all.67), calls=%async_computation.5 | async-start | bytes 524288 | tf_op jit(solution)/shard_map/all_to_all | solution.py:178
  140.9 59.6 %all-reduce.6.cloned.1.call-start = ((), (), s32[]{:S(2)}) async-start(), calls=%async_computation.7 | async-start | bytes 131072
Sparse Core Ops, SparseCore 0:
  64.2 52.5 all-reduce.3
  150.0 50.4 all-reduce.5
where the time goes:
time: 213 us; the launch traced here: 212 us
  waiting for transfers between devices  122 us (57%)
  matrix products  21.2 us (10%)
  starting transfers between devices  19.6 us (9%)
  between operations  16.4 us (8%)
  other arithmetic  12.9 us (6%)
  blocking collectives  12.5 us (6%)
  local copies, waits for them, and re-layouts  7.42 us (3%)
    psum x1, waiting for transfers between devices, on_device(): mixed = lax.psum(head_term.astype(jnp.bfloat16), 'tp').astype(jnp.float32)  52.6 us
    unnamed x3, waiting for transfers between devices  48.9 us
    all_to_all x1, blocking collectives, on_device(): lax.all_to_all(outgoing, 'ep', split_axis=0, concat_axis=0, tiled=True)  12.5 us
    all_to_all x1, waiting for transfers between devices, on_device(): lax.all_to_all(expert_out, 'ep', split_axis=0, concat_axis=0, tiled=True)  7.75 us
    reduce_sum x5, other arithmetic, rms_scale(): jnp.mean(values_f * values_f, axis=-1, keepdims=True) + EPSILON  5.68 us
    all_to_all x1, starting transfers between devices, on_device(): lax.all_to_all(latent_cols, 'tp', split_axis=0, concat_axis=1, tiled=True)  5.2 us
    all_to_all x1, waiting for transfers between devices, on_device(): lax.all_to_all(attended.reshape(seq_count, -1), 'tp', split_axis=1, conca...  4.81 us
    all_to_all x1, waiting for transfers between devices, on_device(): lax.all_to_all(q_latent, 'tp', split_axis=0, concat_axis=1, tiled=True)  4.75 us
  transfers between devices with their start and end apart: 7, of which 6 were waited for; matrix products, arithmetic and copies ran while one was open for 6% of the time, Pallas kernels for 0%

commit v1 on v0

v1 whole, which is shorter than its diff:
```python
import functools
import jax
import jax.numpy as jnp
from jax import lax
from jax.experimental import pallas as pl
from jax.experimental.pallas import tpu as pltpu
from jax.sharding import PartitionSpec as P

EPSILON = 1e-06
ROTARY_BASE = 500000.0
LANES = 128
FOLD = 8
SPLIT = 4
F32 = jnp.float32
BF16 = jnp.bfloat16


def round_up(value, step):
    return (value + step - 1) // step * step


def inv_rms(v):
    return lax.rsqrt(jnp.mean(v * v, axis=-1, keepdims=True) + EPSILON)


def folded_inv_rms(v):
    lanes = jnp.sum(v * v, axis=0, keepdims=True)
    mean = jnp.sum(lanes, axis=1, keepdims=True) / (v.shape[0] * v.shape[1])
    return lax.rsqrt(mean + EPSILON)


def fold(dst, row):
    width = row.shape[1] // FOLD
    for j in range(FOLD):
        dst[j : j + 1, :] = row[:, j * width : (j + 1) * width]


def layer_kernel(
    len_ref,
    routes_ref,
    weights_ref,
    *refs,
):
    hbm = refs[:15]
    hidden_ref, latent_out_ref, rope_out_ref = refs[15:18]
    vm = refs[18:33]
    (
        nrm,
        rot_scr,
        qs_f,
        qs,
        qrx,
        q_f,
        lat_f,
        sc_scr,
        att_f,
        as_,
        arx,
        st,
        val,
        ms,
        mrx,
        tok_row,
        es,
        erx,
        xs_f,
        xs,
        xrx,
        x_f,
        x_b,
        ys,
        yrx,
        rs,
        rrx,
        ms_f,
        gain_f,
        out_row,
        tot_f,
        load_sem,
        part_sem,
        s1,
        r1,
        s2,
        r2,
        s3,
        r3,
        s4,
        r4,
        s5,
        r5,
        s6,
        r6,
        s7,
        r7,
    ) = refs[33:]
    tok, gains, wq, wku, wqr, wld, wrd, lgain, cl, cr, wvu, wo, wg, wu, wd = vm
    T = lax.axis_size("tp")
    E = lax.axis_size("ep")
    me = lax.axis_index("tp")
    grp = lax.axis_index("ep")
    G, D = tok.shape
    H, N, C = wku.shape
    V = wvu.shape[2]
    R = wrd.shape[0]
    CC = wld.shape[1]
    POS = cl.shape[1]
    half = R // 2
    NT = (((1,), (1,)), ((), ()))

    barrier = pltpu.get_barrier_semaphore()

    def greet_tp(i, carry):
        pl.semaphore_signal(
            barrier,
            inc=1,
            device_id={"tp": lax.rem(me + i, T)},
            device_id_type=pl.DeviceIdType.MESH,
        )
        return carry

    def greet_ep(i, carry):
        pl.semaphore_signal(
            barrier,
            inc=1,
            device_id={"ep": lax.rem(grp + i, E)},
            device_id_type=pl.DeviceIdType.MESH,
        )
        return carry

    lax.fori_loop(1, T, greet_tp, 0)
    lax.fori_loop(1, E, greet_ep, 0)

    loads = [pltpu.make_async_copy(hbm[i], vm[i], load_sem.at[i]) for i in range(15)]
    part = D // SPLIT

    def projection_loads(k):
        at = pl.ds(k * part, part)
        return [
            pltpu.make_async_copy(hbm[i].at[at], vm[i].at[at], part_sem.at[i, k])
            for i in (2, 4, 5)
        ]

    for i in (0, 1):
        loads[i].start()
    for k in range(SPLIT):
        for copy in projection_loads(k):
            copy.start()
    for i in (3, 6, 7):
        loads[i].start()
    names = (
        ("tok", "gains", "wq", "wku", "wqr", "wld", "wrd", "lgain")
        + ("cl", "cr", "wvu", "wo", "wg", "wu", "wd")
    )

    def ready(*which):
        for name in which:
            loads[names.index(name)].wait()

    def rdma(axis, src, dst, send, recv, peer):
        return pltpu.make_async_remote_copy(
            src_ref=src,
            dst_ref=dst,
            send_sem=send,
            recv_sem=recv,
            device_id={axis: peer},
            device_id_type=pl.DeviceIdType.MESH,
        )

    def scatter(axis, mine, size, src, dst, send, recv):
        def pick(peer):
            return src.at[peer] if len(src.shape) == len(dst.shape) else src

        def go(i, carry):
            peer = lax.rem(mine + i, size)
            rdma(axis, pick(peer), dst.at[mine], send.at[peer], recv.at[mine], peer).start()
            return carry

        lax.fori_loop(1, size, go, 0)

    def collect(axis, mine, size, src, dst, send, recv):
        def pick(peer):
            return src.at[peer] if len(src.shape) == len(dst.shape) else src

        def go(i, carry):
            peer = lax.rem(mine + i, size)
            copy = rdma(axis, pick(peer), dst.at[peer], send.at[peer], recv.at[peer], peer)
            copy.wait_recv()
            return carry

        lax.fori_loop(1, size, go, 0)

    def drain(axis, mine, size, src, dst, send, recv):
        def pick(peer):
            return src.at[peer] if len(src.shape) == len(dst.shape) else src

        def go(i, carry):
            peer = lax.rem(mine + i, size)
            copy = rdma(axis, pick(peer), dst.at[peer], send.at[peer], recv.at[peer], peer)
            copy.wait_send()
            return carry

        lax.fori_loop(1, size, go, 0)

    def mm_k(x_ref, w_ref, width):
        chunk = min(1024, x_ref.shape[1])

        def step(k, acc):
            at = pl.ds(pl.multiple_of(k * chunk, chunk), chunk)
            return acc + jnp.dot(x_ref[:, at], w_ref[at, :], preferred_element_type=F32)

        return lax.fori_loop(
            0, x_ref.shape[1] // chunk, step, jnp.zeros((x_ref.shape[0], width), F32)
        )

    qs_f[...] = jnp.zeros_like(qs_f)
    rot_scr[...] = jnp.zeros_like(rot_scr)
    lane = lax.broadcasted_iota(jnp.int32, (1, LANES), 1)
    spot = lax.rem(lane, half).astype(F32)
    position = len_ref[0].astype(F32)
    angles = position * jnp.exp(spot * (-jnp.log(jnp.full((1, LANES), ROTARY_BASE, F32)) / half))
    cos_row, sin_row = jnp.cos(angles), jnp.sin(angles)

    def rotate(v):
        turned = jnp.where(
            lane < half,
            -pltpu.roll(v, LANES - half, 1),
            pltpu.roll(v, half, 1),
        )
        return jnp.where(lane < R, v * cos_row + turned * sin_row, 0.0)

    ready("tok", "gains")
    x = tok[...].astype(F32)
    nrm[...] = (x * inv_rms(x) * gains[0:1, :]).astype(BF16)
    rows = lax.broadcasted_iota(jnp.int32, (G, 1), 0)
    fold(tok_row, jnp.sum(jnp.where(rows == me, x, 0.0), axis=0, keepdims=True))
    for j in range(3):
        fold(gain_f.at[j], gains[j + 1 : j + 2, :])

    q_nope = jnp.zeros((G, H * N), F32)
    q_rot = jnp.zeros((G, H * R), F32)
    lat_cols = jnp.zeros((G, CC), F32)
    for k in range(SPLIT):
        for copy in projection_loads(k):
            copy.wait()
        if k == SPLIT // 2:
            for copy in loads[8:]:
                copy.start()
        at = slice(k * part, (k + 1) * part)
        q_nope = q_nope + jnp.dot(nrm[:, at], wq[at, :], preferred_element_type=F32)
        q_rot = q_rot + jnp.dot(nrm[:, at], wqr[at, :], preferred_element_type=F32)
        lat_cols = lat_cols + jnp.dot(nrm[:, at], wld[at, :], preferred_element_type=F32)
    q_nope = q_nope.astype(BF16)
    ready("wku")
    for h in range(H):
        ql = jnp.dot(q_nope[:, h * N : (h + 1) * N], wku[h], preferred_element_type=F32)
        for t in range(G):
            qs_f[t, h : h + 1, 0:C] = ql[t : t + 1, :]
    rot_scr[:, 0 : H * R] = q_rot
    for h in range(H):
        start = h * R // LANES * LANES
        piece = rot_scr[:, start : start + LANES]
        if h * R % LANES:
            piece = pltpu.roll(piece, LANES - h * R % LANES, 1)
        piece = jnp.where(lane < R, piece, 0.0)
        for t in range(G):
            qs_f[t, h : h + 1, C : C + LANES] = piece[t : t + 1, :]
    for t in range(G):
        qs_f[t, 0:1, C + LANES : C + LANES + CC] = lat_cols[t : t + 1, :]
    for t in range(T):
        qs[t] = qs_f[t].astype(BF16)

    pl.semaphore_wait(barrier, T - 1 + E - 1)
    scatter("tp", me, T, qs, qrx, s1, r1)
    qrx[me] = qs[me]

    ready("wrd", "lgain", "cl", "cr")
    rot_scr[...] = jnp.zeros_like(rot_scr)
    rot_scr[:, 0:R] = lax.dot_general(nrm[...], wrd[...], NT, preferred_element_type=F32)
    raw = jnp.sum(jnp.where(rows == me, rot_scr[:, 0:LANES], 0.0), axis=0, keepdims=True)
    rope_new = rotate(raw.astype(BF16).astype(F32)).astype(BF16)
    rope_out_ref[...] = rope_new[:, 0:R]

    collect("tp", me, T, qs, qrx, s1, r1)
    for s in range(T):
        q_f[s * H : (s + 1) * H, :] = qrx[s].astype(F32)
        lat_f[:, s * CC : (s + 1) * CC] = q_f[s * H : s * H + 1, C + LANES : C + LANES + CC]
    lat = lat_f[...]
    lat_new = (lat * inv_rms(lat) * lgain[...]).astype(BF16)
    latent_out_ref[...] = lat_new
    lat_new_f = lat_new.astype(F32)

    q_lat = q_f[:, 0:C]
    q_pe = rotate(q_f[:, C : C + LANES]).astype(BF16)
    q_lat_b = q_lat.astype(BF16)
    scale = (N + R) ** (-0.5)
    pos_chunk = min(256, POS)
    q_pe_b = q_pe[:, 0:R]

    def score_step(p, carry):
        at = pl.ds(pl.multiple_of(p * pos_chunk, pos_chunk), pos_chunk)
        sc_scr[:, at] = lax.dot_general(
            q_lat_b, cl[0, at, :], NT, preferred_element_type=F32
        ) + jnp.dot(q_pe_b, cr[0, :, at], preferred_element_type=F32)
        return carry

    lax.fori_loop(0, POS // pos_chunk, score_step, 0)
    own_score = (
        jnp.sum(q_lat * lat_new_f, axis=-1, keepdims=True)
        + jnp.sum(q_pe.astype(F32) * rope_new.astype(F32), axis=-1, keepdims=True)
    ) * scale
    scores = sc_scr[...] * scale
    visible = lax.broadcasted_iota(jnp.int32, scores.shape, 1) < len_ref[0]
    row_max = jnp.maximum(
        jnp.max(jnp.where(visible, scores, -jnp.inf), axis=-1, keepdims=True), own_score
    )
    exps = jnp.where(visible, jnp.exp(scores - row_max), 0.0)
    own_exp = jnp.exp(own_score - row_max)
    denominator = jnp.sum(exps, axis=-1, keepdims=True) + own_exp
    probs = (exps / denominator).astype(BF16)
    own_prob = (own_exp / denominator).astype(BF16).astype(F32)
    lat_f[...] = lat_new_f
    lat_chunk = min(256, C)

    def attend_step(c, carry):
        at = pl.ds(pl.multiple_of(c * lat_chunk, lat_chunk), lat_chunk)
        att_f[:, at] = (
            jnp.dot(probs, cl[0, :, at], preferred_element_type=F32) + own_prob * lat_f[:, at]
        )
        return carry

    lax.fori_loop(0, C // lat_chunk, attend_step, 0)
    for s in range(T):
        as_[s] = att_f[s * H : (s + 1) * H, :].astype(BF16)
    scatter("tp", me, T, as_, arx, s2, r2)
    arx[me] = as_[me]
    ready("wvu", "wo")
    collect("tp", me, T, as_, arx, s2, r2)

    for t in range(T):
        block = arx[t].astype(F32)
        for h in range(H):
            st[h, t : t + 1, :] = block[h : h + 1, :]
    for h in range(H):
        val[:, h * V : (h + 1) * V] = jnp.dot(
            st[h].astype(BF16), wvu[h], preferred_element_type=F32
        ).astype(BF16)
    width = D // FOLD
    for j in range(FOLD):
        part_out = jnp.dot(
            val[...], wo[:, j * width : (j + 1) * width], preferred_element_type=F32
        )
        for t in range(G):
            ms_f[t, j : j + 1, :] = part_out[t : t + 1, :]
    for t in range(G):
        ms[t] = ms_f[t].astype(BF16)
    scatter("tp", me, T, ms, mrx, s3, r3)
    mrx[me] = ms[me]
    collect("tp", me, T, ms, mrx, s3, r3)
    mixed = mrx[0].astype(F32)
    for s in range(1, T):
        mixed = mixed + mrx[s].astype(F32)
    resid = tok_row[...] + mixed * folded_inv_rms(mixed) * gain_f[0]
    resid = resid.astype(BF16).astype(F32)
    tok_row[...] = resid
    expert_in = (resid * folded_inv_rms(resid) * gain_f[1]).astype(BF16)
    es[...] = expert_in
    scatter("ep", grp, E, es, erx, s4, r4)
    erx[grp] = expert_in
    collect("ep", grp, E, es, erx, s4, r4)
    for e in range(E):
        row = erx[e].astype(F32)
        for j in range(FOLD):
            xs_f[e : e + 1, j * width : (j + 1) * width] = row[j : j + 1, :]
    xs[...] = xs_f[...].astype(BF16)
    scatter("tp", me, T, xs, xrx, s5, r5)
    xrx[me] = xs[...]
    ready("wg", "wu", "wd")
    collect("tp", me, T, xs, xrx, s5, r5)
    for s in range(T):
        x_f[s * E : (s + 1) * E, :] = xrx[s].astype(F32)
    x_b[...] = x_f[...].astype(BF16)

    F = wg.shape[2]
    gate = mm_k(x_b, wg.at[0], F)
    up = mm_k(x_b, wu.at[0], F)
    hidden = (gate / (1.0 + jnp.exp(-gate)) * up).astype(BF16)

    out_chunk = min(1024, D)

    def down_step(n, carry):
        at = pl.ds(pl.multiple_of(n * out_chunk, out_chunk), out_chunk)
        x_f[:, at] = jnp.dot(hidden, wd[0, :, at], preferred_element_type=F32)
        return carry

    lax.fori_loop(0, D // out_chunk, down_step, 0)
    for s in range(T):
        ys[s] = x_f[s * E : (s + 1) * E, :].astype(BF16)
    scatter("tp", me, T, ys, yrx, s6, r6)
    yrx[me] = ys[me]
    collect("tp", me, T, ys, yrx, s6, r6)
    total = yrx[0].astype(F32)
    for s in range(1, T):
        total = total + yrx[s].astype(F32)
    for e in range(E):
        fold(tot_f, total[e : e + 1, :])
        rs[e] = tot_f[...].astype(BF16)
    scatter("ep", grp, E, rs, rrx, s7, r7)
    rrx[grp] = rs[grp]
    collect("ep", grp, E, rs, rrx, s7, r7)
    routed = jnp.zeros((FOLD, width), F32)
    for e in range(E):
        weight = jnp.float32(0.0)
        for k in range(routes_ref.shape[0]):
            weight = weight + jnp.where(routes_ref[k, me] == e, weights_ref[k, me], 0.0)
        routed = routed + weight * rrx[e].astype(F32)
    out = tok_row[...] + routed * folded_inv_rms(routed) * gain_f[2]
    for j in range(FOLD):
        out_row[:, j * width : (j + 1) * width] = out[j : j + 1, :]
    hidden_ref[...] = out_row[...].astype(BF16)

    drain("tp", me, T, qs, qrx, s1, r1)
    drain("tp", me, T, as_, arx, s2, r2)
    drain("tp", me, T, ms, mrx, s3, r3)
    drain("ep", grp, E, es, erx, s4, r4)
    drain("tp", me, T, xs, xrx, s5, r5)
    drain("tp", me, T, ys, yrx, s6, r6)
    drain("ep", grp, E, rs, rrx, s7, r7)


def on_device(
    tokens,
    norm_gains,
    w_query,
    w_query_rope,
    w_key_up,
    w_value_up,
    w_output,
    w_latent_down,
    latent_gain,
    w_rope_down,
    cache_latent,
    cache_rope,
    lengths,
    routes,
    route_weights,
    w_gate,
    w_up,
    w_down,
):
    T = lax.axis_size("tp")
    E = lax.axis_size("ep")
    G, D = tokens.shape
    H, N, C = w_key_up.shape
    V = w_value_up.shape[2]
    R = w_rope_down.shape[1]
    CC = w_latent_down.shape[1]
    POS = cache_latent.shape[1]
    W = C + LANES + round_up(CC, LANES)
    loaded = (
        tokens,
        norm_gains,
        w_query,
        w_key_up,
        w_query_rope,
        w_latent_down,
        w_rope_down.T,
        latent_gain.reshape(1, -1),
        cache_latent,
        jnp.swapaxes(cache_rope, 1, 2),
        w_value_up,
        w_output,
        w_gate,
        w_up,
        w_down,
    )
    sem = pltpu.SemaphoreType.DMA
    scratch = [pltpu.VMEM(a.shape, a.dtype) for a in loaded] + [
        pltpu.VMEM((G, D), BF16),
        pltpu.VMEM((G, round_up(H * R, LANES)), F32),
        pltpu.VMEM((T, H, W), F32),
        pltpu.VMEM((T, H, W), BF16),
        pltpu.VMEM((T, H, W), BF16),
        pltpu.VMEM((T * H, W), F32),
        pltpu.VMEM((1, C), F32),
        pltpu.VMEM((T * H, POS), F32),
        pltpu.VMEM((T * H, C), F32),
        pltpu.VMEM((T, H, C), BF16),
        pltpu.VMEM((T, H, C), BF16),
        pltpu.VMEM((H, G, C), F32),
        pltpu.VMEM((G, H * V), BF16),
        pltpu.VMEM((T, FOLD, D // FOLD), BF16),
        pltpu.VMEM((T, FOLD, D // FOLD), BF16),
        pltpu.VMEM((FOLD, D // FOLD), F32),
        pltpu.VMEM((FOLD, D // FOLD), BF16),
        pltpu.VMEM((E, FOLD, D // FOLD), BF16),
        pltpu.VMEM((E, D), F32),
        pltpu.VMEM((E, D), BF16),
        pltpu.VMEM((T, E, D), BF16),
        pltpu.VMEM((T * E, D), F32),
        pltpu.VMEM((T * E, D), BF16),
        pltpu.VMEM((T, E, D), BF16),
        pltpu.VMEM((T, E, D), BF16),
        pltpu.VMEM((E, FOLD, D // FOLD), BF16),
        pltpu.VMEM((E, FOLD, D // FOLD), BF16),
        pltpu.VMEM((T, FOLD, D // FOLD), F32),
        pltpu.VMEM((3, FOLD, D // FOLD), F32),
        pltpu.VMEM((1, D), F32),
        pltpu.VMEM((FOLD, D // FOLD), F32),
        sem((len(loaded),)),
        sem((len(loaded), SPLIT)),
        sem((T,)),
        sem((T,)),
        sem((T,)),
        sem((T,)),
        sem((T,)),
        sem((T,)),
        sem((E,)),
        sem((E,)),
        sem((T,)),
        sem((T,)),
        sem((T,)),
        sem((T,)),
        sem((E,)),
        sem((E,)),
    ]
    smem = pl.BlockSpec(memory_space=pltpu.SMEM)
    vmem = pl.BlockSpec(memory_space=pltpu.VMEM)
    anywhere = pl.BlockSpec(memory_space=pl.ANY)
    return pl.pallas_call(
        layer_kernel,
        out_shape=(
            jax.ShapeDtypeStruct((1, D), BF16),
            jax.ShapeDtypeStruct((1, C), BF16),
            jax.ShapeDtypeStruct((1, R), BF16),
        ),
        in_specs=[smem] * 3 + [anywhere] * len(loaded),
        out_specs=(vmem,) * 3,
        scratch_shapes=scratch,
        compiler_params=pltpu.CompilerParams(
            collective_id=0, has_side_effects=True, vmem_limit_bytes=60 * 1024 * 1024
        ),
    )(lengths, routes.T, route_weights.T, *loaded)


def solution(mesh):
    in_specs = (
        P("ep", None),
        P(),
        P(None, "tp"),
        P(None, "tp"),
        P("tp", None, None),
        P("tp", None, None),
        P("tp", None),
        P(None, "tp"),
        P(),
        P(),
        P(("ep", "tp"), None, None),
        P(("ep", "tp"), None, None),
        P(("ep", "tp")),
        P("ep", None),
        P("ep", None),
        P("ep", None, "tp"),
        P("ep", None, "tp"),
        P("ep", "tp", None),
    )
    out_specs = (P(("ep", "tp"), None), P(("ep", "tp"), None), P(("ep", "tp"), None))
    return jax.shard_map(
        on_device, mesh=mesh, in_specs=in_specs, out_specs=out_specs, check_vma=False
    )
```

time: 213 us -> 47.9 us (0.22)
  waiting for transfers between devices: 122 us -> 0 us
  Pallas kernels: 0 us -> 42.5 us
  matrix products: 21.2 us -> 0 us
  starting transfers between devices: 19.6 us -> 0 us
  between operations: 16.4 us -> 1.29 us
  other arithmetic: 12.9 us -> 0 us
  blocking collectives: 12.5 us -> 0 us
  local copies, waits for them, and re-layouts: 7.42 us -> 3.79 us
    psum x1 -> x0, waiting for transfers between devices: 52.6 us -> none  [on_device(): mixed = lax.psum(head_term.astype(jnp.bfloat16), 'tp').astype(jnp.float32)]
    unnamed x3 -> x0, waiting for transfers between devices: 48.9 us -> none
    pallas_call x0 -> x1, Pallas kernels: none -> 42.5 us  [on_device(): pl.pallas_call(layer_kernel, out_shape=(jax.ShapeDtypeStruct((1, D), BF16...]
    dot_general x15 -> x0, matrix products: 21.2 us -> none  [the longest x1 3.68 us: on_device(): head_term = jnp.dot(values, w_output, preferred_element_type=jnp.float32)]
    all_to_all x5 -> x0, waiting for transfers between devices: 20.6 us -> none  [the longest x1 7.75 us: on_device(): lax.all_to_all(expert_out, 'ep', split_axis=0, concat_axis=0, tiled=True)]
    all_to_all x5 -> x0, starting transfers between devices: 19.5 us -> none  [the longest x1 5.2 us: on_device(): lax.all_to_all(latent_cols, 'tp', split_axis=0, concat_axis=1, tiled=True)]
    all_to_all x1 -> x0, blocking collectives: 12.5 us -> none  [on_device(): lax.all_to_all(outgoing, 'ep', split_axis=0, concat_axis=0, tiled=True)]
    reduce_sum x8 -> x0, other arithmetic: 6.15 us -> none  [the longest x5 5.68 us: rms_scale(): jnp.mean(values_f * values_f, axis=-1, keepdims=True) + EPSILON]
  transfers between devices with their start and end apart: 7 -> 0, of which waited for: 6 -> 0; matrix products, arithmetic and copies ran while one was open for 6% -> 0% of each run, Pallas kernels for 0% -> 0%
where the time goes in v1:
time: 47.9 us; the launch traced here: 47.6 us
  Pallas kernels  42.5 us (89%)
  local copies, waits for them, and re-layouts  3.79 us (8%)
  between operations  1.29 us (3%)
    pallas_call x1, Pallas kernels, on_device(): pl.pallas_call(layer_kernel, out_shape=(jax.ShapeDtypeStruct((1, D), BF16...  42.5 us
    unnamed x3, local copies, waits for them, and re-layouts  3.79 us

profile of v1, /device:TPU:0, one launch (start us, length us, event | category | flops | bytes accessed | tf_op | source)
XLA Modules:
  0.0 47.6 jit_solution(2553592349283180856)
XLA Ops:
  1.3 42.5 %shard_map.193 = (bf16[1,4096]{1,0:T(2,128)(2,1)}, bf16[1,1024]{1,0:T(2,128)(2,1)}, bf16[1,64]{1,0:T(2,128)(2,1)}) custom-call(s32[1]{0:T(128)S(6)} %copy.24.len_ref, s32[2,8]{1,0:T(2,128)} %bitcast.8, f32[2,8]{1,0:T(2,128)} %bitcast.9, bf16[8,4096]{1,0:T(8,128)(2,1)} %refs_0_.1, f32[4,4096]{1,0:T(4,128)} %refs_1_.1, bf16[4096,512]{1,0:T(8,128)(2,1)} %refs_2_.1, ...), custom_call_target="tpu_custom_call" | custom-call | tf_op jit(solution)/shard_map/pallas_call | solution.py:529
  43.8 1.3 %copy.25 = bf16[1,4096]{1,0:T(2,128)(2,1)} copy(bf16[1,4096]{1,0:T(2,128)(2,1)} %get-tuple-element.6) | data formatting | bytes 16384
  45.1 1.3 %copy.26 = bf16[1,1024]{1,0:T(2,128)(2,1)} copy(bf16[1,1024]{1,0:T(2,128)(2,1)} %get-tuple-element.7) | data formatting | bytes 4096
  46.4 1.2 %copy.27 = bf16[1,64]{1,0:T(2,128)(2,1)} copy(bf16[1,64]{1,0:T(2,128)(2,1)} %get-tuple-element.8) | data formatting | bytes 256

commit v2 on v1

--- a/solution.py
+++ b/solution.py
@@ -425,6 +425,12 @@
     drain("tp", me, T, xs, xrx, s5, r5)
     drain("tp", me, T, ys, yrx, s6, r6)
     drain("ep", grp, E, rs, rrx, s7, r7)
+
+
+def hand_over(*refs):
+    count = len(refs) // 2
+    for source, target in zip(refs[:count], refs[count:]):
+        target[...] = source[...]
 
 
 def on_device(
@@ -526,13 +532,10 @@
     smem = pl.BlockSpec(memory_space=pltpu.SMEM)
     vmem = pl.BlockSpec(memory_space=pltpu.VMEM)
     anywhere = pl.BlockSpec(memory_space=pl.ANY)
-    return pl.pallas_call(
+    shapes = tuple(jax.ShapeDtypeStruct((1, n), BF16) for n in (D, C, R))
+    results = pl.pallas_call(
         layer_kernel,
-        out_shape=(
-            jax.ShapeDtypeStruct((1, D), BF16),
-            jax.ShapeDtypeStruct((1, C), BF16),
-            jax.ShapeDtypeStruct((1, R), BF16),
-        ),
+        out_shape=shapes,
         in_specs=[smem] * 3 + [anywhere] * len(loaded),
         out_specs=(vmem,) * 3,
         scratch_shapes=scratch,
@@ -540,6 +543,9 @@
             collective_id=0, has_side_effects=True, vmem_limit_bytes=60 * 1024 * 1024
         ),
     )(lengths, routes.T, route_weights.T, *loaded)
+    return pl.pallas_call(
+        hand_over, out_shape=shapes, in_specs=[vmem] * 3, out_specs=(vmem,) * 3
+    )(*results)
 
 
 def solution(mesh):

time: 47.9 us -> 45.3 us (0.946)
  local copies, waits for them, and re-layouts: 3.79 us -> 0 us
  Pallas kernels: 42.5 us -> 43.8 us
    unnamed x3 -> x0, local copies, waits for them, and re-layouts: 3.79 us -> none
    pallas_call x1 -> x2, Pallas kernels: 42.5 us -> 43.8 us  [the longest x1 42.5 us: on_device(): pl.pallas_call(layer_kernel, out_shape=shapes, in_specs=[smem] * 3 + [any...]
where the time goes in v2:
time: 45.3 us; the launch traced here: 45.1 us
  Pallas kernels  43.8 us (97%)
  between operations  1.29 us (3%)
    pallas_call x1, Pallas kernels, on_device(): pl.pallas_call(layer_kernel, out_shape=shapes, in_specs=[smem] * 3 + [any...  42.5 us
    pallas_call x1, Pallas kernels, on_device(): pl.pallas_call(hand_over, out_shape=shapes, in_specs=[vmem] * 3, out_spec...  1.35 us

profile of v2, /device:TPU:0, one launch (start us, length us, event | category | flops | bytes accessed | tf_op | source)
XLA Modules:
  0.0 45.1 jit_solution(4345988839313322606)
XLA Ops:
  1.3 42.5 %shard_map.193 = (bf16[1,4096]{1,0:T(2,128)(2,1)}, bf16[1,1024]{1,0:T(2,128)(2,1)}, bf16[1,64]{1,0:T(2,128)(2,1)}) custom-call(s32[1]{0:T(128)S(6)} %copy.21.len_ref, s32[2,8]{1,0:T(2,128)} %bitcast.8, f32[2,8]{1,0:T(2,128)} %bitcast.9, bf16[8,4096]{1,0:T(8,128)(2,1)} %refs_0_.1, f32[4,4096]{1,0:T(4,128)} %refs_1_.1, bf16[4096,512]{1,0:T(8,128)(2,1)} %refs_2_.1, ...), custom_call_target="tpu_custom_call" | custom-call | tf_op jit(solution)/shard_map/pallas_call | solution.py:536
  43.8 1.3 %shard_map.194 = (bf16[1,4096]{1,0:T(2,128)(2,1)}, bf16[1,1024]{1,0:T(2,128)(2,1)}, bf16[1,64]{1,0:T(2,128)(2,1)}) custom-call(bf16[1,4096]{1,0:T(2,128)(2,1)} %get-tuple-element.6.refs_0_, bf16[1,1024]{1,0:T(2,128)(2,1)} %get-tuple-element.7.refs_1_, bf16[1,64]{1,0:T(2,128)(2,1)} %get-tuple-element.8.refs_2_), custom_call_target="tpu_custom_call" | custom-call | tf_op jit(solution)/shard_map/pallas_call | solution.py:546
